TPU v7x, 512 devices: a 8x2x16 block of a 8x8x16 slice. The times are simulated.
512 devices in a mesh: grp: 2 (over y), fs: 32 (over z, core), tp: 8 (over x).
Axes of the slice: x: 8, y: 2, z: 16, core: 2. Of those that a mesh axis runs over, the one named last changes fastest.
The devices are a block of a 8x8x16 slice.
Arguments:
- tokens: bfloat16 [24576, 2048], P(('grp', 'fs'), 'tp'), parts along dimension 0, may hold values from -6 to 6
- norm_gain: float32 [2048], P('fs'), may hold values from 0.1 to 1.9
- gate_weight: float32 [32, 2048, 1024], P(None, 'fs', 'tp'), may hold values from -0.125 to 0.125
- up_weight: float32 [32, 2048, 1024], P(None, 'fs', 'tp'), may hold values from -0.125 to 0.125
- down_weight: float32 [32, 1024, 2048], P(None, 'fs', 'tp'), may hold values from -0.1875 to 0.1875
- routes: int32 [24576, 2], P(('grp', 'fs')), parts along dimension 0, may hold values from 0 to 31, as said below
- route_weights: float32 [24576, 2], P(('grp', 'fs')), parts along dimension 0, may hold values from 0.2 to 1
Outputs:
- gate_serve: bfloat16 [64, 2048, 1024], P(('grp', 'fs'), None, 'tp'), parts along dimension 0
- up_serve: bfloat16 [64, 2048, 1024], P(('grp', 'fs'), None, 'tp'), parts along dimension 0
- down_serve: bfloat16 [64, 1024, 2048], P(('grp', 'fs'), None, 'tp'), parts along dimension 0
- mixture: bfloat16 [24576, 2048], P(('grp', 'fs'), 'tp'), parts along dimension 0
There are 2 independent parts, one for each index of `grp`. A program takes and returns all parts, laid end to end along the dimension named above; an argument that names none is the same for every part. Nothing has to cross between parts.
Inputs may be any that keep to these rules, and one draw needn't show every extreme that they name: `routes`: each row names two different experts of one group (expert e lies in group e // 8). In each aligned block of 384 rows no expert is named more than 36 times, and every expert of one group is named exactly 36 times.
All inputs are finite; a program needn't handle non-finite values.
Results may differ from a plain program's by a relative error of at most 0.0087.
Values may be sent and summed in bfloat16 or wider, within the bound.
No kernel may reach another device: no remote copies, remote signals or barrier semaphores. Data moves between devices by JAX's collectives and lax.ppermute only.
A program may use at most 64 MiB of HBM per device.

v0:
```python
import jax
import jax.numpy as jnp
from jax import lax
from jax.sharding import Mesh
from jax.sharding import PartitionSpec as P

CAP = 36
FS = ("fs_0", "fs_1")
GRP_FS = ("grp", "fs_0", "fs_1")
epsilon = 1e-06


def in_blocks(x, dim, length):
    before, after = (x.shape[:dim], x.shape[dim + 1 :])
    return jnp.moveaxis(x.reshape(*before, length, -1, *after), dim, 0)


def laid_out(blocks, dim):
    blocks = jnp.moveaxis(blocks, 0, dim)
    shape = blocks.shape
    return blocks.reshape(*shape[:dim], shape[dim] * shape[dim + 1], *shape[dim + 2 :])


def exchange_in_order(blocks, axes, order):
    shape = [lax.axis_size(a) for a in axes]
    blocks = blocks.reshape(*shape, *blocks.shape[1:])
    for k in order:
        blocks = lax.all_to_all(blocks, axes[k], split_axis=k, concat_axis=k, tiled=True)
    return blocks.reshape(-1, *blocks.shape[len(axes) :])


def exchange_by_chip(x, groups, order, split_dim, concat_dim):
    length = lax.axis_size(groups[0]) * lax.axis_size(groups[1])
    blocks = in_blocks(x, split_dim, length)
    return laid_out(exchange_in_order(blocks, groups, order), concat_dim)


def normalize(rows):
    values = rows.astype(jnp.float32)
    scale = lax.rsqrt(jnp.mean(values * values, axis=-1, keepdims=True) + epsilon)
    return (values * scale).astype(jnp.bfloat16)


def shards(tokens, norm_gain, gate_weight, up_weight, down_weight, routes, route_weights):
    experts = gate_weight.shape[0]
    n_shards = lax.axis_size(FS)
    local_experts = experts // n_shards
    tok_rows = tokens.shape[0]
    gate_low = (norm_gain[None, :, None] * gate_weight).astype(jnp.bfloat16)
    up_low = (norm_gain[None, :, None] * up_weight).astype(jnp.bfloat16)
    down_low = down_weight.astype(jnp.bfloat16)
    gate_serve, up_serve = (
        lax.all_to_all(gate_low, FS, split_axis=0, concat_axis=1, tiled=True),
        lax.all_to_all(up_low, FS, split_axis=0, concat_axis=1, tiled=True),
    )
    flat_routes = routes.reshape(-1)
    expert_ids = lax.iota(jnp.int32, experts)
    onehot = (flat_routes[:, None] == expert_ids[None, :]).astype(jnp.int32)
    position = jnp.sum((jnp.cumsum(onehot, axis=0) - 1) * onehot, axis=1)
    slot_index = (flat_routes * CAP + position).reshape(tok_rows, 2)
    slot_ids = lax.iota(jnp.int32, experts * CAP)
    select = jnp.any(slot_ids[:, None, None] == slot_index[None, :, :], axis=2).astype(jnp.bfloat16)
    outbound = jnp.dot(select, tokens, preferred_element_type=jnp.float32).astype(jnp.bfloat16)
    outbound = outbound.reshape(n_shards, local_experts, CAP, outbound.shape[1])
    arrived = lax.all_to_all(outbound, FS, split_axis=0, concat_axis=2, tiled=True)[0]
    expert_rows = normalize(lax.all_gather(arrived, "tp", axis=2, tiled=True))
    gate_part = jnp.einsum(
        "erd,edh->erh", expert_rows, gate_serve, preferred_element_type=jnp.float32
    )
    up_part = jnp.einsum("erd,edh->erh", expert_rows, up_serve, preferred_element_type=jnp.float32)
    hidden = (jax.nn.silu(gate_part) * up_part).astype(jnp.bfloat16)
    down_serve = lax.all_to_all(down_low, FS, split_axis=0, concat_axis=1, tiled=True)
    expert_out = jnp.einsum(
        "erk,ekd->erd",
        lax.all_gather(hidden, "tp", axis=2, tiled=True),
        down_serve,
        preferred_element_type=jnp.float32,
    ).astype(jnp.bfloat16)
    expert_out = expert_out.reshape(1, local_experts, hidden.shape[1], expert_out.shape[2])
    returned_rows = exchange_by_chip(expert_out, ("fs_0", "fs_1"), (1, 0), 2, 0)
    returned_rows = returned_rows.reshape(experts * CAP, returned_rows.shape[3])
    picked = returned_rows[slot_index]
    mixture = jnp.sum(route_weights[:, :, None] * picked.astype(jnp.float32), axis=1).astype(
        jnp.bfloat16
    )
    return (gate_serve, up_serve, down_serve, mixture)


def solution(mesh):
    split = Mesh(
        mesh.devices.reshape(mesh.shape["grp"], 16, 2, mesh.shape["tp"]),
        ("grp", "fs_0", "fs_1", "tp"),
    )
    placed = (
        P(GRP_FS, "tp"),
        P(FS),
        P(None, FS, "tp"),
        P(None, FS, "tp"),
        P(None, FS, "tp"),
        P(GRP_FS, None),
        P(GRP_FS, None),
    )
    return jax.shard_map(
        shards,
        mesh=split,
        in_specs=placed,
        out_specs=(
            P(GRP_FS, None, "tp"),
            P(GRP_FS, None, "tp"),
            P(GRP_FS, None, "tp"),
            P(GRP_FS, "tp"),
        ),
        check_vma=False,
    )
```

profile of v0, /device:TPU:66, one launch (start us, length us, event | category | flops | bytes accessed | tf_op | source)
XLA Modules:
  0.0 293.5 jit_solution(14518242084303444602)
XLA Ops:
  7.3 0.9 copy.41
  8.5 1.7 reduce-window.6
  10.3 0.3 slice_reduce_fusion
  10.7 0.2 reduce_sum.30
  10.9 0.7 compare_select_fusion
  11.6 0.8 fusion.3
  12.4 0.5 convolution_convert_fusion.1
  13.0 82.9 %all_to_all.55 = bf16[32,1,36,256]{3,2,1,0:T(8,128)(2,1)S(1)} all-to-all(bf16[32,1,36,256]{3,2,1,0:T(8,128)(2,1)S(1)} %bitcast.35), channel_id=1, replica_groups=mesh['grp'=2,'fs_0'=16,'fs_1'=2,'tp'=8] {'fs_0','fs_1'}, dimensions={0} | all-to-all | bytes 1179648 | tf_op jit(solution)/shard_map/all_to_all | solution.py:65
  95.9 0.9 squeeze.3
  96.9 2.3 multiply_convert_fusion
  99.2 37.1 %all_to_all.56 = bf16[32,64,128]{2,1,0:T(8,128)(2,1)S(1)} all-to-all(bf16[32,64,128]{2,1,0:T(8,128)(2,1)S(1)} %get-tuple-element.7), channel_id=1, replica_groups=mesh['grp'=2,'fs_0'=16,'fs_1'=2,'tp'=8] {'fs_0','fs_1'}, dimensions={0} | all-to-all | bytes 1048576 | tf_op jit(solution)/shard_map/all_to_all | solution.py:53
  136.3 4.8 %all-to-all-start.1 = ((bf16[32,64,128]{2,1,0:T(8,128)(2,1)}), bf16[32,64,128]{2,1,0:T(8,128)(2,1)S(1)}, u32[]{:S(2)}, u32[]{:S(2)}) async-start(bf16[32,64,128]{2,1,0:T(8,128)(2,1)} %get-tuple-element.6), calls=%async_computation.1 | async-start | bytes 1048576 | tf_op jit(solution)/shard_map/all_to_all | solution.py:54
  141.2 22.0 %all-gather.4.cloned.1.call-done = bf16[1,1152,2048]{2,1,0:T(8,128)(2,1)} async-done(((bf16[1,1152,256]{2,1,0:T(8,128)(2,1)}), bf16[1,1152,2048]{2,1,0:T(8,128)(2,1)}) %all-gather.4.cloned.1.call-update) | async-done | bytes 4718608 | tf_op jit(solution)/shard_map/all_gather | solution.py:66
  163.2 3.5 %fusion = f32[1152]{0:T(1024)S(1)} fusion(bf16[1,1152,2048]{2,1,0:T(8,128)(2,1)} %all-gather.4.cloned.1.call-done), kind=kLoop, calls=%fused_computation.3 | loop fusion | flops 7076736 | bytes 4723200 | tf_op jit(solution)/shard_map/reduce_sum | solution.py:40
  166.7 0.3 copy-done.1
  167.0 1.5 fusion.6
  168.5 5.8 %all-to-all-done.1 = bf16[32,64,128]{2,1,0:T(8,128)(2,1)S(1)} async-done(((bf16[32,64,128]{2,1,0:T(8,128)(2,1)}), bf16[32,64,128]{2,1,0:T(8,128)(2,1)S(1)}, u32[]{:S(2)}, u32[]{:S(2)}) %all-to-all-start.1) | async-done | bytes 524320 | tf_op jit(solution)/shard_map/all_to_all | solution.py:54
  174.3 4.6 %fusion.4 = bf16[1152,128]{1,0:T(8,128)(2,1)} fusion(bf16[2048,128]{1,0:T(8,128)(2,1)S(1)} %bitcast.38, bf16[1,1152,2048]{2,1,0:T(8,128)(2,1)} %all-gather.4.cloned.1.call-done, f32[1152]{0:T(1024)S(1)} %add_rsqrt_fusion, f32[1152,128]{1,0:T(8,128)S(1)} %fusion.6), kind=kOutput, calls=%fused_computation.11 | convolution fusion | flops 611942400 | bytes 6132224 | tf_op jit(solution)/shard_map/erd,edh->erh/dot_general | solution.py:70
  179.0 38.7 %all_to_all.57 = bf16[32,32,256]{2,1,0:T(8,128)(2,1)S(1)} all-to-all(bf16[32,32,256]{2,1,0:T(8,128)(2,1)S(1)} %convert_element_type.42), channel_id=1, replica_groups=mesh['grp'=2,'fs_0'=16,'fs_1'=2,'tp'=8] {'fs_0','fs_1'}, dimensions={0} | all-to-all | bytes 1048576 | tf_op jit(solution)/shard_map/all_to_all | solution.py:72
  217.8 9.2 %all-gather.6.cloned.1.call-done = bf16[1152,1024]{1,0:T(8,128)(2,1)} async-done(((bf16[1152,128]{1,0:T(8,128)(2,1)}), bf16[1152,1024]{1,0:T(8,128)(2,1)}) %all-gather.6.cloned.1.call-update) | async-done | bytes 2359312 | tf_op jit(solution)/shard_map/all_gather | solution.py:75
  226.9 2.4 convolution_convert_fusion
  229.5 0.2 copy.46
  229.7 4.2 %all_to_all.58 = bf16[16,2,1,1,36,256]{5,0,4,3,2,1:T(8,128)(2,1)S(1)} all-to-all(bf16[16,2,1,1,36,256]{5,0,4,3,2,1:T(8,128)(2,1)S(1)} %copy.46), channel_id=1, replica_groups=mesh['grp'=2,'fs_0'=16,'fs_1'=2,'tp'=8] {'fs_1'}, dimensions={1} | all-to-all | bytes 1179648 | tf_op jit(solution)/shard_map/all_to_all | solution.py:28
  233.9 1.4 copy.47
  235.3 13.1 %all-to-all-start.5 = ((bf16[16,2,1,1,36,256]{5,1,4,3,2,0:T(2,128)(2,1)}), bf16[16,2,1,1,36,256]{5,1,4,3,2,0:T(2,128)(2,1)S(1)}, u32[]{:S(2)}, u32[]{:S(2)}) async-start(bf16[16,2,1,1,36,256]{5,1,4,3,2,0:T(2,128)(2,1)} %copy.47), calls=%async_computation.5 | async-start | bytes 1179648 | tf_op jit(solution)/shard_map/all_to_all | solution.py:28
  248.9 30.4 %all-to-all-done.5 = bf16[16,2,1,1,36,256]{5,1,4,3,2,0:T(2,128)(2,1)S(1)} async-done(((bf16[16,2,1,1,36,256]{5,1,4,3,2,0:T(2,128)(2,1)}), bf16[16,2,1,1,36,256]{5,1,4,3,2,0:T(2,128)(2,1)S(1)}, u32[]{:S(2)}, u32[]{:S(2)}) %all-to-all-start.5) | async-done | bytes 589856 | tf_op jit(solution)/shard_map/all_to_all | solution.py:28
  279.5 2.7 gather_fusion
  282.1 0.4 reshape.117
  282.5 1.7 multiply_reduce_fusion
  284.2 0.8 copy.55
  285.0 0.8 copy.56
  285.8 0.8 copy.57
  (31 shorter events, 1.7 us)
Async XLA Ops:
  7.2 5.2 %copy-start = (bf16[384,256]{1,0:T(8,128)(2,1)S(1)}, bf16[384,256]{1,0:T(8,128)(2,1)}, u32[]{:S(2)}) copy-start(bf16[384,256]{1,0:T(8,128)(2,1)} %param.7) | copy-start | bytes 589828
  7.2 89.7 %copy-start.3 = (f32[32,64,128]{2,1,0:T(8,128)S(1)}, f32[32,64,128]{2,1,0:T(8,128)}, u32[]{:S(2)}) copy-start(f32[32,64,128]{2,1,0:T(8,128)} %param.10) | copy-start | bytes 3145732
  7.2 89.7 %copy-start.5 = (f32[64]{0:T(128)S(1)}, f32[64]{0:T(128)}, u32[]{:S(2)}) copy-start(f32[64]{0:T(128)} %param.8) | copy-start | bytes 772
  7.2 156.0 %all-gather.4.cloned.1.call-start = ((), (), s32[]{:S(2)}) async-start(), calls=%async_computation.6 | async-start | bytes 5308416 | tf_op jit(solution)/shard_map/all_gather | solution.py:66
  136.3 38.0 %all-to-all-start.1 = ((bf16[32,64,128]{2,1,0:T(8,128)(2,1)}), bf16[32,64,128]{2,1,0:T(8,128)(2,1)S(1)}, u32[]{:S(2)}, u32[]{:S(2)}) async-start(bf16[32,64,128]{2,1,0:T(8,128)(2,1)} %get-tuple-element.6), calls=%async_computation.1 | async-start | bytes 1048576 | tf_op jit(solution)/shard_map/all_to_all | solution.py:54
  141.1 85.8 %all-gather.6.cloned.1.call-start = ((), (), s32[]{:S(2)}) async-start(), calls=%async_computation.7 | async-start | bytes 2654208 | tf_op jit(solution)/shard_map/all_gather | solution.py:75
  163.2 3.8 %copy-start.1 = (bf16[1,1152,2048]{2,1,0:T(8,128)(2,1)S(1)}, bf16[1,1152,2048]{2,1,0:T(8,128)(2,1)}, u32[]{:S(2)}) copy-start(bf16[1,1152,2048]{2,1,0:T(8,128)(2,1)} %all-gather.4.cloned.1.call-done) | copy-start | bytes 14155780
  174.3 4.7 %copy-start.2 = (f32[32,32,256]{2,1,0:T(8,128)S(1)}, f32[32,32,256]{2,1,0:T(8,128)}, u32[]{:S(2)}) copy-start(f32[32,32,256]{2,1,0:T(8,128)} %param.11) | copy-start | bytes 3145732
  229.4 19.4 %copy-start.4 = (f32[384,2]{0,1:T(2,128)S(1)}, f32[384,2]{0,1:T(2,128)}, u32[]{:S(2)}) copy-start(f32[384,2]{0,1:T(2,128)} %param.13) | copy-start | bytes 9220
  235.3 43.9 %all-to-all-start.5 = ((bf16[16,2,1,1,36,256]{5,1,4,3,2,0:T(2,128)(2,1)}), bf16[16,2,1,1,36,256]{5,1,4,3,2,0:T(2,128)(2,1)S(1)}, u32[]{:S(2)}, u32[]{:S(2)}) async-start(bf16[16,2,1,1,36,256]{5,1,4,3,2,0:T(2,128)(2,1)} %copy.47), calls=%async_computation.5 | async-start | bytes 1179648 | tf_op jit(solution)/shard_map/all_to_all | solution.py:28
Sparse Core Ops, SparseCore 0:
  97.0 66.1 all-gather.3
  179.1 47.8 all-gather.5
where the time goes:
time: 294 us; the launch traced here: 293 us
  blocking collectives  163 us (55%)
  waiting for transfers between devices  67.5 us (23%)
  starting transfers between devices  18 us (6%)
  between operations  14.3 us (5%)
  other arithmetic  10.9 us (4%)
  local copies, waits for them, and re-layouts  10.8 us (4%)
  matrix products  8.96 us (3%)
    all_to_all x1, blocking collectives, shards(): lax.all_to_all(outbound, FS, split_axis=0, concat_axis=2, tiled=True)[0]  82.9 us
    all_to_all x1, blocking collectives, shards(): lax.all_to_all(down_low, FS, split_axis=0, concat_axis=1, tiled=True)  38.7 us
    all_to_all x1, blocking collectives, shards(): lax.all_to_all(gate_low, FS, split_axis=0, concat_axis=1, tiled=True)  37.1 us
    all_to_all x1, waiting for transfers between devices, exchange_in_order(): lax.all_to_all(blocks, axes[k], split_axis=k, concat_axis=k, tiled=True)  30.4 us
    all_gather x1, waiting for transfers between devices, shards(): expert_rows = normalize(lax.all_gather(arrived, 'tp', axis=2, tiled=True))  22 us
    all_to_all x1, starting transfers between devices, exchange_in_order(): lax.all_to_all(blocks, axes[k], split_axis=k, concat_axis=k, tiled=True)  13.1 us
    all_gather x1, waiting for transfers between devices, shards(): lax.all_gather(hidden, 'tp', axis=2, tiled=True)  9.16 us
  transfers between devices with their start and end apart: 4, of which 4 were waited for; matrix products, arithmetic and copies ran while one was open for 3% of the time, Pallas kernels for 0%

commit v1 on v0

--- a/solution.py
+++ b/solution.py
@@ -50,7 +50,10 @@
     up_low = (norm_gain[None, :, None] * up_weight).astype(jnp.bfloat16)
     down_low = down_weight.astype(jnp.bfloat16)
     gate_serve, up_serve = (
-        lax.all_to_all(gate_low, FS, split_axis=0, concat_axis=1, tiled=True),
+        jnp.concatenate(
+            lax.all_to_all(jnp.stack(jnp.split(gate_low, lax.axis_size(FS), axis=0)), FS, 0, 0),
+            axis=1,
+        ),
         lax.all_to_all(up_low, FS, split_axis=0, concat_axis=1, tiled=True),
     )
     flat_routes = routes.reshape(-1)

time: 294 us -> 295 us (level)
  blocking collectives: 163 us -> 82 us
  starting transfers between devices: 18 us -> 62.5 us
  waiting for transfers between devices: 67.5 us -> 104 us
    all_to_all x2 -> x1, blocking collectives: 120 us -> 37.1 us  [shards(): lax.all_to_all(jnp.stack(jnp.split(gate_low, lax.axis_size(FS), axis=0)),...]
    all_to_all x0 -> x1, starting transfers between devices: none -> 44.4 us  [shards(): lax.all_to_all(outbound, FS, split_axis=0, concat_axis=2, tiled=True)[0]]
    all_to_all x0 -> x1, waiting for transfers between devices: none -> 37.4 us  [shards(): lax.all_to_all(outbound, FS, split_axis=0, concat_axis=2, tiled=True)[0]]
  transfers between devices with their start and end apart: 4 -> 5, of which waited for: 4 -> 5; matrix products, arithmetic and copies ran while one was open for 3% -> 2% of each run, Pallas kernels for 0% -> 0%
where the time goes in v1:
time: 295 us; the launch traced here: 294 us
  waiting for transfers between devices  104 us (35%)
  blocking collectives  82 us (28%)
  starting transfers between devices  62.5 us (21%)
  between operations  14.4 us (5%)
  local copies, waits for them, and re-layouts  12 us (4%)
  other arithmetic  9.78 us (3%)
  matrix products  8.98 us (3%)
    all_to_all x1, starting transfers between devices, shards(): lax.all_to_all(outbound, FS, split_axis=0, concat_axis=2, tiled=True)[0]  44.4 us
    all_to_all x1, blocking collectives, shards(): lax.all_to_all(down_low, FS, split_axis=0, concat_axis=1, tiled=True)  40.7 us
    all_to_all x1, waiting for transfers between devices, shards(): lax.all_to_all(outbound, FS, split_axis=0, concat_axis=2, tiled=True)[0]  37.4 us
    all_to_all x1, blocking collectives, shards(): lax.all_to_all(jnp.stack(jnp.split(gate_low, lax.axis_size(FS), axis=0)),...  37.1 us
    all_to_all x1, waiting for transfers between devices, exchange_in_order(): lax.all_to_all(blocks, axes[k], split_axis=k, concat_axis=k, tiled=True)  30.4 us
    all_gather x1, waiting for transfers between devices, shards(): expert_rows = normalize(lax.all_gather(arrived, 'tp', axis=2, tiled=True))  23.6 us
    all_to_all x1, starting transfers between devices, exchange_in_order(): lax.all_to_all(blocks, axes[k], split_axis=k, concat_axis=k, tiled=True)  13.1 us
    all_gather x1, waiting for transfers between devices, shards(): lax.all_gather(hidden, 'tp', axis=2, tiled=True)  8.71 us
  transfers between devices with their start and end apart: 5, of which 5 were waited for; matrix products, arithmetic and copies ran while one was open for 2% of the time, Pallas kernels for 0%

profile of v1, /device:TPU:66, one launch (start us, length us, event | category | flops | bytes accessed | tf_op | source)
XLA Modules:
  0.0 294.1 jit_solution(4648277082027423270)
XLA Ops:
  7.2 1.0 copy.41
  8.5 1.7 reduce-window.6
  10.3 0.3 slice_reduce_fusion
  10.9 0.7 compare_select_fusion
  11.6 0.8 fusion.3
  12.4 0.5 convolution_convert_fusion.1
  12.9 1.0 reshape.100
  13.8 44.4 %all-to-all-start.3 = ((bf16[32,1,36,256]{3,2,1,0:T(8,128)(2,1)}), bf16[32,1,36,256]{3,2,1,0:T(8,128)(2,1)S(1)}, u32[]{:S(2)}, u32[]{:S(2)}) async-start(bf16[32,1,36,256]{3,2,1,0:T(8,128)(2,1)} %bitcast.36), calls=%async_computation.3 | async-start | bytes 1310720 | tf_op jit(solution)/shard_map/all_to_all | solution.py:68
  58.4 1.1 multiply_convert_fusion
  59.6 37.4 %all-to-all-done.3 = bf16[32,1,36,256]{3,2,1,0:T(8,128)(2,1)S(1)} async-done(((bf16[32,1,36,256]{3,2,1,0:T(8,128)(2,1)}), bf16[32,1,36,256]{3,2,1,0:T(8,128)(2,1)S(1)}, u32[]{:S(2)}, u32[]{:S(2)}) %all-to-all-start.3) | async-done | bytes 589856 | tf_op jit(solution)/shard_map/all_to_all | solution.py:68
  97.0 0.9 squeeze.3
  98.3 37.1 %all_to_all.48 = bf16[32,1,64,128]{3,2,1,0:T(8,128)(2,1)S(1)} all-to-all(bf16[32,1,64,128]{3,2,1,0:T(8,128)(2,1)S(1)} %constant_dynamic-update-slice_fusion), channel_id=1, replica_groups=mesh['grp'=2,'fs_0'=16,'fs_1'=2,'tp'=8] {'fs_0','fs_1'}, dimensions={0} | all-to-all | bytes 1048576 | tf_op jit(solution)/shard_map/all_to_all | solution.py:54
  135.4 4.8 %all-to-all-start.1 = ((bf16[32,64,128]{2,1,0:T(8,128)(2,1)}), bf16[32,64,128]{2,1,0:T(8,128)(2,1)S(1)}, u32[]{:S(2)}, u32[]{:S(2)}) async-start(bf16[32,64,128]{2,1,0:T(8,128)(2,1)} %get-tuple-element.6), calls=%async_computation.1 | async-start | bytes 1048576 | tf_op jit(solution)/shard_map/all_to_all | solution.py:57
  140.2 23.6 %all-gather.4.cloned.1.call-done = bf16[1,1152,2048]{2,1,0:T(8,128)(2,1)} async-done(((bf16[1,1152,256]{2,1,0:T(8,128)(2,1)}), bf16[1,1152,2048]{2,1,0:T(8,128)(2,1)}) %all-gather.4.cloned.1.call-update) | async-done | bytes 4718608 | tf_op jit(solution)/shard_map/all_gather | solution.py:69
  163.8 3.5 %fusion = f32[1152]{0:T(1024)S(1)} fusion(bf16[1,1152,2048]{2,1,0:T(8,128)(2,1)} %all-gather.4.cloned.1.call-done), kind=kLoop, calls=%fused_computation.3 | loop fusion | flops 7076736 | bytes 4723200 | tf_op jit(solution)/shard_map/reduce_sum | solution.py:40
  167.3 0.3 copy-done.1
  167.6 1.5 fusion.6
  169.1 4.3 %all-to-all-done.1 = bf16[32,64,128]{2,1,0:T(8,128)(2,1)S(1)} async-done(((bf16[32,64,128]{2,1,0:T(8,128)(2,1)}), bf16[32,64,128]{2,1,0:T(8,128)(2,1)S(1)}, u32[]{:S(2)}, u32[]{:S(2)}) %all-to-all-start.1) | async-done | bytes 524320 | tf_op jit(solution)/shard_map/all_to_all | solution.py:57
  173.3 4.6 %fusion.4 = bf16[1152,128]{1,0:T(8,128)(2,1)} fusion(bf16[2048,128]{1,0:T(8,128)(2,1)S(1)} %bitcast.165, bf16[1,1152,2048]{2,1,0:T(8,128)(2,1)} %all-gather.4.cloned.1.call-done, f32[1152]{0:T(1024)S(1)} %add_rsqrt_fusion, f32[1152,128]{1,0:T(8,128)S(1)} %fusion.6), kind=kOutput, calls=%fused_computation.11 | convolution fusion | flops 611942400 | bytes 6132224 | tf_op jit(solution)/shard_map/erd,edh->erh/dot_general | solution.py:73
  178.1 40.7 %all_to_all.49 = bf16[32,32,256]{2,1,0:T(8,128)(2,1)S(1)} all-to-all(bf16[32,32,256]{2,1,0:T(8,128)(2,1)S(1)} %convert_element_type.42), channel_id=1, replica_groups=mesh['grp'=2,'fs_0'=16,'fs_1'=2,'tp'=8] {'fs_0','fs_1'}, dimensions={0} | all-to-all | bytes 1048576 | tf_op jit(solution)/shard_map/all_to_all | solution.py:75
  218.8 8.7 %all-gather.6.cloned.1.call-done = bf16[1152,1024]{1,0:T(8,128)(2,1)} async-done(((bf16[1152,128]{1,0:T(8,128)(2,1)}), bf16[1152,1024]{1,0:T(8,128)(2,1)}) %all-gather.6.cloned.1.call-update) | async-done | bytes 2359312 | tf_op jit(solution)/shard_map/all_gather | solution.py:78
  227.5 2.4 convolution_convert_fusion
  230.3 4.2 %all_to_all.50 = bf16[16,2,1,1,36,256]{5,0,4,3,2,1:T(8,128)(2,1)S(1)} all-to-all(bf16[16,2,1,1,36,256]{5,0,4,3,2,1:T(8,128)(2,1)S(1)} %copy.46), channel_id=1, replica_groups=mesh['grp'=2,'fs_0'=16,'fs_1'=2,'tp'=8] {'fs_1'}, dimensions={1} | all-to-all | bytes 1179648 | tf_op jit(solution)/shard_map/all_to_all | solution.py:28
  234.5 1.4 copy.47
  236.0 13.1 %all-to-all-start.5 = ((bf16[16,2,1,1,36,256]{5,1,4,3,2,0:T(2,128)(2,1)}), bf16[16,2,1,1,36,256]{5,1,4,3,2,0:T(2,128)(2,1)S(1)}, u32[]{:S(2)}, u32[]{:S(2)}) async-start(bf16[16,2,1,1,36,256]{5,1,4,3,2,0:T(2,128)(2,1)} %copy.47), calls=%async_computation.5 | async-start | bytes 1179648 | tf_op jit(solution)/shard_map/all_to_all | solution.py:28
  249.5 30.4 %all-to-all-done.5 = bf16[16,2,1,1,36,256]{5,1,4,3,2,0:T(2,128)(2,1)S(1)} async-done(((bf16[16,2,1,1,36,256]{5,1,4,3,2,0:T(2,128)(2,1)}), bf16[16,2,1,1,36,256]{5,1,4,3,2,0:T(2,128)(2,1)S(1)}, u32[]{:S(2)}, u32[]{:S(2)}) %all-to-all-start.5) | async-done | bytes 589856 | tf_op jit(solution)/shard_map/all_to_all | solution.py:28
  280.1 2.7 gather_fusion
  282.8 0.4 reshape.118
  283.1 1.7 multiply_reduce_fusion
  284.9 0.8 copy.86
  285.7 0.8 copy.87
  286.5 0.8 copy.88
  (66 shorter events, 2.2 us)
Async XLA Ops:
  7.2 5.2 %copy-start = (bf16[384,256]{1,0:T(8,128)(2,1)S(1)}, bf16[384,256]{1,0:T(8,128)(2,1)}, u32[]{:S(2)}) copy-start(bf16[384,256]{1,0:T(8,128)(2,1)} %param.7) | copy-start | bytes 589828
  7.2 51.2 %copy-start.3 = (f32[32,64,128]{2,1,0:T(8,128)S(1)}, f32[32,64,128]{2,1,0:T(8,128)}, u32[]{:S(2)}) copy-start(f32[32,64,128]{2,1,0:T(8,128)} %param.10) | copy-start | bytes 3145732
  7.2 51.2 %copy-start.6 = (f32[64]{0:T(128)S(1)}, f32[64]{0:T(128)}, u32[]{:S(2)}) copy-start(f32[64]{0:T(128)} %param.8) | copy-start | bytes 772
  7.2 51.2 %copy-start.4 = (f32[32,64,128]{2,1,0:T(8,128)S(1)}, f32[32,64,128]{2,1,0:T(8,128)}, u32[]{:S(2)}) copy-start(f32[32,64,128]{2,1,0:T(8,128)} %param.9) | copy-start | bytes 3145732
  13.8 83.1 %all-to-all-start.3 = ((bf16[32,1,36,256]{3,2,1,0:T(8,128)(2,1)}), bf16[32,1,36,256]{3,2,1,0:T(8,128)(2,1)S(1)}, u32[]{:S(2)}, u32[]{:S(2)}) async-start(bf16[32,1,36,256]{3,2,1,0:T(8,128)(2,1)} %bitcast.36), calls=%async_computation.3 | async-start | bytes 1310720 | tf_op jit(solution)/shard_map/all_to_all | solution.py:68
  58.3 105.6 %all-gather.4.cloned.1.call-start = ((), (), s32[]{:S(2)}) async-start(), calls=%async_computation.6 | async-start | bytes 5308416 | tf_op jit(solution)/shard_map/all_gather | solution.py:69
  135.4 38.0 %all-to-all-start.1 = ((bf16[32,64,128]{2,1,0:T(8,128)(2,1)}), bf16[32,64,128]{2,1,0:T(8,128)(2,1)S(1)}, u32[]{:S(2)}, u32[]{:S(2)}) async-start(bf16[32,64,128]{2,1,0:T(8,128)(2,1)} %get-tuple-element.6), calls=%async_computation.1 | async-start | bytes 1048576 | tf_op jit(solution)/shard_map/all_to_all | solution.py:57
  140.2 87.4 %all-gather.6.cloned.1.call-start = ((), (), s32[]{:S(2)}) async-start(), calls=%async_computation.7 | async-start | bytes 2654208 | tf_op jit(solution)/shard_map/all_gather | solution.py:78
  163.8 3.8 %copy-start.1 = (bf16[1,1152,2048]{2,1,0:T(8,128)(2,1)S(1)}, bf16[1,1152,2048]{2,1,0:T(8,128)(2,1)}, u32[]{:S(2)}) copy-start(bf16[1,1152,2048]{2,1,0:T(8,128)(2,1)} %all-gather.4.cloned.1.call-done) | copy-start | bytes 14155780
  173.3 4.7 %copy-start.2 = (f32[32,32,256]{2,1,0:T(8,128)S(1)}, f32[32,32,256]{2,1,0:T(8,128)}, u32[]{:S(2)}) copy-start(f32[32,32,256]{2,1,0:T(8,128)} %param.11) | copy-start | bytes 3145732
  230.0 19.4 %copy-start.5 = (f32[384,2]{0,1:T(2,128)S(1)}, f32[384,2]{0,1:T(2,128)}, u32[]{:S(2)}) copy-start(f32[384,2]{0,1:T(2,128)} %param.13) | copy-start | bytes 9220
  236.0 43.9 %all-to-all-start.5 = ((bf16[16,2,1,1,36,256]{5,1,4,3,2,0:T(2,128)(2,1)}), bf16[16,2,1,1,36,256]{5,1,4,3,2,0:T(2,128)(2,1)S(1)}, u32[]{:S(2)}, u32[]{:S(2)}) async-start(bf16[16,2,1,1,36,256]{5,1,4,3,2,0:T(2,128)(2,1)} %copy.47), calls=%async_computation.5 | async-start | bytes 1179648 | tf_op jit(solution)/shard_map/all_to_all | solution.py:28
Sparse Core Ops, SparseCore 0:
  98.1 65.7 all-gather.3
  178.1 49.3 all-gather.5
